TPU v7x, 32 devices: a whole 2x2x4 slice. The times are simulated.
32 devices in a mesh: kv: 8 (over z, y), tp: 4 (over x, core).
Axes of the slice: x: 2, y: 2, z: 4, core: 2. Of those that a mesh axis runs over, the one named last changes fastest.
Arguments:
- tokens: bfloat16 [1024, 4096], P(None, 'kv'), may hold values from -6 to 6
- norm_gain: float32 [4096], replicated, may hold values from 0.1 to 1.9
- query_weight: bfloat16 [4096, 2048], P('kv', 'tp'), may hold values from -0.09375 to 0.09375
- key_weight: bfloat16 [4096, 2048], P('kv', 'tp'), may hold values from -0.09375 to 0.09375
- value_weight: bfloat16 [4096, 4096], P('kv', 'tp'), may hold values from -0.09375 to 0.09375
- outgate_weight: bfloat16 [4096, 4096], P('kv', 'tp'), may hold values from -0.09375 to 0.09375
- gate_weight: bfloat16 [4096, 32], P('kv'), may hold values from -0.09375 to 0.09375
- forget_bias: float32 [16], replicated, may hold values from -1 to 5
- head_gain: float32 [4096], P('tp'), may hold values from 0.1 to 1.9
- output_weight: bfloat16 [4096, 4096], P('tp', 'kv'), may hold values from -0.09375 to 0.09375
- state_matrix: float32 [256, 16, 128, 256], P('kv', 'tp'), may hold values from -6 to 6
- state_normal: float32 [256, 16, 128], P('kv', 'tp'), may hold values from -6 to 6
- state_stable: float32 [256, 16], P('kv', 'tp'), may hold values from -3 to 3
- prior_keys: bfloat16 [256, 4, 2048], P('kv', None, 'tp'), may hold values from -0.59765625 to 0.59765625
- prior_values: bfloat16 [256, 4, 4096], P('kv', None, 'tp'), may hold values from -6 to 6
- prior_ingate: float32 [256, 4, 16], P('kv', None, 'tp'), may hold values from -4 to 4
- prior_forget: float32 [256, 4, 16], P('kv', None, 'tp'), may hold values from -2 to -0.02
- accepted: int32 [256], P('kv'), may hold values from 0 to 4
- parents: int32 [256, 4], P('kv'), may hold values from -1 to 2, as said below
Outputs:
- layer_out: bfloat16 [1024, 4096], P('tp', 'kv')
- new_matrix: float32 [256, 16, 128, 256], P('kv', 'tp')
- new_normal: float32 [256, 16, 128], P('kv', 'tp')
- new_stable: float32 [256, 16], P('kv', 'tp')
Inputs may be any that keep to these rules, and one draw needn't show every extreme that they name: parents of proposal t lie in -1 to t - 1; the first proposal's parent is -1; in some sequence each proposal's parent is the one before it.
All inputs are finite; a program needn't handle non-finite values.
Results may differ from a plain program's by a relative error of at most 0.0089.
Values may be sent and summed in bfloat16 or wider, within the bound.
A program may use at most 128 MiB of HBM per device.

v0:
```python
import functools

import jax
import jax.numpy as jnp
from jax import lax
from jax.experimental import pallas as pl
from jax.experimental.pallas import tpu as pltpu
from jax.sharding import PartitionSpec as P

D = 4096
HEADS = 16
DQK = 128
DV = 256
PROP = 4
LANES = 128
NEG = -1e30
F32 = jnp.float32
BF16 = jnp.bfloat16
HP = lax.Precision.HIGHEST


def ancestry(parents):
    count = parents.shape[1]
    index = jnp.arange(count, dtype=jnp.int32)
    current = jnp.broadcast_to(index[None, :], parents.shape)
    table = jnp.broadcast_to(
        (index[:, None] == index[None, :]).astype(F32), (parents.shape[0], count, count)
    )
    for repeat in range(count - 1):
        hit = current[:, :, None] == index[None, None, :]
        looked = jnp.sum(jnp.where(hit, parents[:, None, :], 0), axis=2)
        current = jnp.where(current >= 0, looked, -1)
        table = table + (current[:, :, None] == index[None, None, :]).astype(F32)
    return table


def commit_kernel(seqs, heads, decay_ref, m_ref, k_ref, v_ref, w_ref, out_ref, low_ref):
    step = pl.program_id(0)
    rows = seqs * PROP
    row_seq = lax.broadcasted_iota(jnp.int32, (rows, 1), 0) // PROP
    for h in range(heads):
        keys = k_ref[:, h * DQK : (h + 1) * DQK].astype(F32)
        vals = v_ref[:, h * DV : (h + 1) * DV].astype(F32) * w_ref[:, h : h + 1]
        lead = vals.astype(BF16)
        rest = (vals - lead.astype(F32)).astype(BF16)
        both = jnp.concatenate([lead, rest], axis=0)
        for s in range(seqs):
            own = jnp.where(row_seq == s, keys, 0.0).astype(BF16)
            added = lax.dot_general(
                jnp.concatenate([own, own], axis=0),
                both,
                (((0,), (0,)), ((), ())),
                preferred_element_type=F32,
            )
            new = decay_ref[step * seqs + s, h] * m_ref[s, h] + added
            out_ref[s, h] = new
            low_ref[s, h] = new.astype(BF16)


def commit_matrix(decay, matrix, keys, values, weights, seqs):
    total, heads, _, _ = matrix.shape
    rows = seqs * PROP
    block = pl.BlockSpec((seqs, heads, DQK, DV), lambda i: (i, 0, 0, 0))
    return pl.pallas_call(
        functools.partial(commit_kernel, seqs, heads),
        grid=(total // seqs,),
        out_shape=[
            jax.ShapeDtypeStruct(matrix.shape, F32),
            jax.ShapeDtypeStruct(matrix.shape, BF16),
        ],
        in_specs=[
            pl.BlockSpec(memory_space=pltpu.SMEM),
            block,
            pl.BlockSpec((rows, heads * DQK), lambda i: (i, 0)),
            pl.BlockSpec((rows, heads * DV), lambda i: (i, 0)),
            pl.BlockSpec((rows, LANES), lambda i: (i, 0)),
        ],
        out_specs=[block, block],
        cost_estimate=pl.CostEstimate(
            flops=2 * matrix.size * 8, bytes_accessed=matrix.size * 10, transcendentals=0
        ),
        name="commit",
    )(decay, matrix, keys, values, weights)


def read_kernel(
    heads, sq_lane, q_ref, rest_ref, gates_ref, m_ref, table_ref, stable_ref, normal_ref,
    bias_ref, gain_ref, out_ref,
):
    rows = out_ref.shape[0]
    gates = gates_ref[...]
    scale = lax.rsqrt(gates[:, sq_lane : sq_lane + 1] * (1.0 / D) + 1e-06)
    gates = scale * gates
    x = gates + bias_ref[...]
    logforget = jnp.minimum(x, 0.0) - jnp.log1p(jnp.exp(-jnp.abs(x)))
    table = table_ref[...]
    path = jnp.dot(table, logforget, precision=HP, preferred_element_type=F32)
    lifted = pltpu.roll(gates, heads, 1) - path
    pick = (
        lax.broadcasted_iota(jnp.int32, (8, LANES), 1)
        == lax.broadcasted_iota(jnp.int32, (8, LANES), 0) + heads
    ).astype(F32)
    flat = lax.dot_general(
        pick, lifted, (((1,), (1,)), ((), ())), precision=HP, preferred_element_type=F32
    )
    carried_all = path + stable_ref[...]
    row16 = lax.broadcasted_iota(jnp.int32, (16, 1), 0) // PROP
    key_scale = scale / jnp.sqrt(jnp.float32(DQK))
    at_value = heads * DQK
    at_gate = at_value + heads * DV
    for h in range(heads):
        query = scale * q_ref[:, h * DQK : (h + 1) * DQK]
        value = scale * rest_ref[:, at_value + h * DV : at_value + (h + 1) * DV]
        key = key_scale * rest_ref[:, h * DQK : (h + 1) * DQK]
        outgate = scale * rest_ref[:, at_gate + h * DV : at_gate + (h + 1) * DV]
        dlog = path[:, heads + h : heads + h + 1] + flat[h : h + 1, :]
        dlog = jnp.where(table > 0.5, dlog, NEG)
        carried = carried_all[:, heads + h : heads + h + 1]
        top = jnp.maximum(carried, jnp.max(dlog, axis=1, keepdims=True))
        scores = lax.dot_general(
            query, key, (((1,), (1,)), ((), ())), precision=HP, preferred_element_type=F32
        ) * jnp.exp(dlog - top)
        factor = jnp.exp(carried - top)
        low = query.astype(BF16)
        pieces = []
        for g in range(rows // 16):
            part = low[g * 16 : (g + 1) * 16]
            got = None
            for j in range(16 // PROP):
                res = jnp.dot(
                    part, m_ref[g * (16 // PROP) + j, h], preferred_element_type=F32
                )
                got = res if got is None else jnp.where(row16 == j, res, got)
            pieces.append(got)
        from_state = jnp.concatenate(pieces, axis=0)
        numer = (
            jnp.dot(scores, value, precision=HP, preferred_element_type=F32)
            + factor * from_state
        )
        denom = jnp.sum(scores, axis=1, keepdims=True) + factor * jnp.sum(
            query * normal_ref[:, h * DQK : (h + 1) * DQK], axis=1, keepdims=True
        )
        read = numer / jnp.maximum(jnp.abs(denom), jnp.exp(-top))
        normer = lax.rsqrt(jnp.mean(read * read, axis=1, keepdims=True) + 1e-06)
        hidden = (
            read
            * normer
            * gain_ref[:, h * DV : (h + 1) * DV]
            * (1.0 / (1.0 + jnp.exp(-outgate)))
        )
        out_ref[:, h * DV : (h + 1) * DV] = hidden.astype(BF16)


def tree_read(query, rest, gates, sq_lane, matrix, table, stable, normal, bias, gain, rows):
    heads = matrix.shape[1]
    total = query.shape[0]
    seqs = rows // PROP

    def by_row(a):
        return pl.BlockSpec((rows, a.shape[1]), lambda i: (i, 0))

    def whole(a):
        return pl.BlockSpec(a.shape, lambda i: (0, 0))

    return pl.pallas_call(
        functools.partial(read_kernel, heads, sq_lane),
        grid=(total // rows,),
        out_shape=jax.ShapeDtypeStruct((total, heads * DV), BF16),
        in_specs=[by_row(a) for a in (query, rest, gates)]
        + [
            pl.BlockSpec((seqs, heads, DQK, DV), lambda i: (i, 0, 0, 0)),
            pl.BlockSpec((rows, rows), lambda i: (i, 0)),
            by_row(stable),
            by_row(normal),
            whole(bias),
            whole(gain),
        ],
        out_specs=pl.BlockSpec((rows, heads * DV), lambda i: (i, 0)),
        cost_estimate=pl.CostEstimate(
            flops=8 * matrix.size, bytes_accessed=matrix.size * 2, transcendentals=0
        ),
        name="tree_read",
    )(query, rest, gates, matrix, table, stable, normal, bias, gain)


def remote(src, dst, send_sem, recv_sem, kv_index, tp_index):
    return pltpu.make_async_remote_copy(
        src_ref=src,
        dst_ref=dst,
        send_sem=send_sem,
        recv_sem=recv_sem,
        device_id=(kv_index, tp_index),
        device_id_type=pl.DeviceIdType.MESH,
    )


def greet(others):
    barrier = pltpu.get_barrier_semaphore()
    for other in others:
        pl.semaphore_signal(
            barrier, inc=1, device_id=other, device_id_type=pl.DeviceIdType.MESH
        )
    pl.semaphore_wait(barrier, len(others))


def spread_kernel(
    ny, nz, tp, cuts, hid_ref, w_ref, out_ref, held, parts, landed, total,
    up_sem, down_sem, side_sem, got_sem, part_sem, land_sem,
):
    me = lax.axis_index("kv")
    mine = lax.axis_index("tp")
    z, y = me // ny, lax.rem(me, ny)
    kv = ny * nz
    per = kv // tp
    rows = hid_ref.shape[0]
    piece = rows // cuts
    greet(
        [((z + d) % nz * ny + y, mine) for d in sorted({1 % nz, nz - 1}) if d]
        + [(z * ny + (y + d) % ny, mine) for d in range(1, ny)]
        + [(me, (mine + d) % tp) for d in range(1, tp)]
    )

    def slab(b, c):
        return held.at[b, pl.ds(c * piece, piece)]

    def source(s, b, c):
        return hid_ref.at[pl.ds(c * piece, piece)] if s == 0 else slab(b, c)

    def up(s, b, c):
        return remote(source(s, b, c), slab(b, c), up_sem.at[s, c], got_sem.at[b, c], me + ny, mine)

    def down(s, b, c):
        return remote(source(s, b, c), slab(b, c), down_sem.at[s, c], got_sem.at[b, c], me - ny, mine)

    def side(s, b, c, d, way):
        return remote(
            source(s, b, c), slab(b, c), side_sem.at[way, s, d - 1, c], got_sem.at[b, c],
            z * ny + (y + d) % ny, mine,
        )

    def arrive(b, c):
        return remote(slab(b, c), slab(b, c), part_sem.at[b], got_sem.at[b, c], me, mine)

    def product(s, b):
        value = hid_ref[...] if s == 0 else held[b]
        got = jnp.dot(value, w_ref[...], preferred_element_type=F32)
        owner = b // per
        slot = b % per

        @pl.when(owner == mine)
        def _():
            total[slot] = got

        @pl.when(owner != mine)
        def _():
            parts[b] = got.astype(BF16)
            hand(b).start()

    def hand(b):
        owner = b // per
        slot = ((mine + tp - owner) % tp + tp - 1) % tp * per + b % per
        return remote(parts.at[b], landed.at[slot], part_sem.at[b], land_sem.at[slot], me, owner)

    for c in range(cuts):
        @pl.when(z < nz - 1)
        def _():
            up(0, me, c).start()

        @pl.when(z > 0)
        def _():
            down(0, me, c).start()

        for d in range(1, ny):
            side(0, me, c, d, 0).start()
    product(0, me)

    def from_side(s, way):
        base = (z - s + nz) % nz * ny if way == 0 else (z + s) % nz * ny
        for d in range(1, ny):
            b = base + (y + d) % ny
            for c in range(cuts):
                arrive(b, c).wait_recv()
            product(1, b)

    def ways(s):
        return [(0, z - s >= 0)] if s == 0 else [(0, z - s >= 0), (1, z + s < nz)]

    for s in range(1, nz):
        for way, there in ways(s):
            b = ((z - s + nz) % nz if way == 0 else (z + s) % nz) * ny + y

            @pl.when(there)
            def _():
                for c in range(cuts):
                    arrive(b, c).wait_recv()
                    if s < nz - 1:
                        if way == 0:
                            @pl.when(z < nz - 1)
                            def _():
                                up(s, b, c).start()
                        else:
                            @pl.when(z > 0)
                            def _():
                                down(s, b, c).start()
                    for d in range(1, ny):
                        side(s, b, c, d, way).start()
                product(s, b)

        for way, there in ways(s - 1):
            @pl.when(there)
            def _():
                from_side(s - 1, way)

    for way, there in ways(nz - 1):
        @pl.when(there)
        def _():
            from_side(nz - 1, way)

    for slot in range(per):
        acc = total[slot]
        for d in range(1, tp):
            at = (d - 1) * per + slot
            remote(landed.at[at], landed.at[at], part_sem.at[0], land_sem.at[at], me, mine).wait_recv()
            acc = acc + landed[at].astype(F32)
        out_ref[slot * rows : (slot + 1) * rows] = acc.astype(BF16)

    for s in range(nz):
        for way, there in ways(s):
            b = ((z - s + nz) % nz if way == 0 else (z + s) % nz) * ny + y

            @pl.when(there)
            def _():
                for c in range(cuts):
                    if s < nz - 1:
                        if way == 0:
                            @pl.when(z < nz - 1)
                            def _():
                                up(s, b, c).wait_send()
                        if way == 1 or s == 0:
                            @pl.when(z > 0)
                            def _():
                                down(s, b, c).wait_send()
                    for d in range(1, ny):
                        side(s, b, c, d, way).wait_send()
    for b in range(kv):
        @pl.when(b // per != mine)
        def _():
            hand(b).wait_send()


def spread_out(hidden, weight, ny, nz, tp):
    rows, width = hidden.shape
    cols = weight.shape[1]
    kv = ny * nz
    per = kv // tp
    cuts = 2
    vmem = pl.BlockSpec(memory_space=pltpu.VMEM)
    dma = pltpu.SemaphoreType.DMA
    return pl.pallas_call(
        functools.partial(spread_kernel, ny, nz, tp, cuts),
        out_shape=jax.ShapeDtypeStruct((per * rows, cols), BF16),
        in_specs=[vmem, vmem],
        out_specs=vmem,
        scratch_shapes=[
            pltpu.VMEM((kv, rows, width), BF16),
            pltpu.VMEM((kv, rows, cols), BF16),
            pltpu.VMEM(((tp - 1) * per, rows, cols), BF16),
            pltpu.VMEM((per, rows, cols), F32),
            dma((nz, cuts)),
            dma((nz, cuts)),
            dma((2, nz, max(ny - 1, 1), cuts)),
            dma((kv, cuts)),
            dma((kv,)),
            dma(((tp - 1) * per,)),
        ],
        compiler_params=pltpu.CompilerParams(collective_id=0, has_side_effects=True),
        cost_estimate=pl.CostEstimate(
            flops=2 * kv * rows * width * cols, bytes_accessed=8 * rows * width, transcendentals=0
        ),
        name="spread",
    )(hidden, weight)


def gather_sums_kernel(
    ny, nz, lag, tok_hbm, gain_ref, gate_ref, q_hbm, k_hbm, v_hbm, o_hbm,
    q_out, rest_out, gates_out,
    tok, normed, wq, wrest, flat,
    side_out, side_in, line_out, below, above, last_out, last_in,
    flat_out, flat_below, flat_above, flat_last_out, flat_last_in,
    load_sem, side_sem, side_got, line_sem, below_got, above_got, last_sem, last_got,
    fline_sem, fbelow_got, fabove_got, flast_sem, flast_got,
):
    me = lax.axis_index("kv")
    mine = lax.axis_index("tp")
    z, y = me // ny, lax.rem(me, ny)
    rows = q_out.shape[0]
    width = wq.shape[1]
    chunks = wrest.shape[0]
    plane = ny * rows
    units = ny + chunks

    loads = [
        pltpu.make_async_copy(tok_hbm, tok, load_sem.at[0]),
        pltpu.make_async_copy(q_hbm, wq, load_sem.at[1]),
    ]
    for n, (w, at) in enumerate(
        [(w, at) for w in (k_hbm, v_hbm, o_hbm) for at in range(0, w.shape[1], width)]
    ):
        loads.append(
            pltpu.make_async_copy(w.at[:, pl.ds(at, width)], wrest.at[n], load_sem.at[2 + n])
        )
    for load in loads:
        load.start()
    greet(
        [((z + d) % nz * ny + y, mine) for d in sorted({1 % nz, nz - 1}) if d]
        + [(z * ny + (y + d) % ny, mine) for d in range(1, ny)]
    )
    loads[0].wait()

    def prepare(n, carry):
        at = pl.ds(pl.multiple_of(n * rows, rows), rows)
        x = tok[at, :].astype(F32)
        low = (x * gain_ref[...]).astype(BF16)
        normed[at, :] = low
        squares = lax.dot_general(
            jnp.ones((8, x.shape[1]), F32), x * x, (((1,), (1,)), ((), ())),
            precision=HP, preferred_element_type=F32,
        )
        gates = lax.dot_general(
            gate_ref[...], low, (((1,), (1,)), ((), ())), preferred_element_type=F32
        )
        flat[n] = jnp.concatenate([gates, squares], axis=0)
        return carry

    lax.fori_loop(0, ny * nz, prepare, 0)
    for load in loads[1:]:
        load.wait()

    def term(block, w):
        at = pl.ds(pl.multiple_of(block * rows, rows), rows)
        return jnp.dot(normed[at, :], w, preferred_element_type=F32)

    def side(d, p, j):
        u = p * chunks + j
        return remote(
            side_out.at[d - 1, u], side_in.at[ny - d - 1, u], side_sem.at[d - 1, u],
            side_got.at[ny - d - 1, u], z * ny + (y + d) % ny, mine,
        )

    def line(going_up, slot):
        got, sem, far = (below, below_got, me + ny) if going_up else (above, above_got, me - ny)
        return remote(line_out.at[slot], got.at[slot], line_sem.at[slot], sem.at[slot], far, mine)

    def flat_line(going_up, b):
        got, sem, far = (
            (flat_below, fbelow_got, me + ny) if going_up else (flat_above, fabove_got, me - ny)
        )
        return remote(flat_out.at[b], got.at[b], fline_sem.at[b], sem.at[b], far, mine)

    def last(d):
        return remote(
            last_out.at[d - 1], last_in.at[ny - d - 1], last_sem.at[d - 1],
            last_got.at[ny - d - 1], z * ny + (y + d) % ny, mine,
        )

    def flat_last(d):
        return remote(
            flat_last_out.at[d - 1], flat_last_in.at[ny - d - 1], flast_sem.at[d - 1],
            flast_got.at[ny - d - 1], z * ny + (y + d) % ny, mine,
        )

    def arrived(ref, sem):
        remote(ref, ref, load_sem.at[0], sem, me, mine).wait_recv()

    def send_side(p, j):
        for d in range(1, ny):
            side_out[d - 1, p * chunks + j] = term(p * ny + (y + d) % ny, wrest[j]).astype(BF16)
            side(d, p, j).start()

    def side_round(n, carry):
        i, j = n // chunks, n % chunks

        @pl.when(nz - 1 - i > z)
        def _():
            send_side(nz - 1 - i, j)

        @pl.when(i < z)
        def _():
            send_side(i, j)

        return carry

    def side_own(j, carry):
        send_side(z, j)
        return carry

    def with_sides(acc, p, j):
        for d in range(1, ny):
            u = p * chunks + j
            arrived(side_in.at[d - 1, u], side_got.at[d - 1, u])
            acc = acc + side_in[d - 1, u].astype(F32)
        return acc

    def pass_on(going_up, acc, slot):
        got, sem = (below, below_got) if going_up else (above, above_got)
        first = z == 0 if going_up else z == nz - 1

        @pl.when(first)
        def _():
            line_out[slot] = acc.astype(BF16)

        @pl.when(jnp.logical_not(first))
        def _():
            arrived(got.at[slot], sem.at[slot])
            line_out[slot] = (acc + got[slot].astype(F32)).astype(BF16)

        line(going_up, slot).start()

    def pass_flat(going_up, b):
        got, sem = (flat_below, fbelow_got) if going_up else (flat_above, fabove_got)
        first = z == 0 if going_up else z == nz - 1

        @pl.when(first)
        def _():
            flat_out[b] = flat[b]

        @pl.when(jnp.logical_not(first))
        def _():
            arrived(got.at[b], sem.at[b])
            flat_out[b] = flat[b] + got[b]

        flat_line(going_up, b).start()

    early = (nz - 1) * ny
    total = early + (nz - 1) * chunks

    def plane_of(going_up, i):
        return nz - 1 - i if going_up else i

    def flow(going_up, n):
        @pl.when(jnp.logical_and(n >= 0, n < early))
        def _():
            p = plane_of(going_up, n // ny)

            @pl.when(p > z if going_up else p < z)
            def _():
                b = p * ny + n % ny
                pass_flat(going_up, b)
                pass_on(going_up, term(b, wq[...]), p * units + n % ny)

        @pl.when(jnp.logical_and(n >= early, n < total))
        def _():
            p = plane_of(going_up, (n - early) // chunks)
            j = (n - early) % chunks

            @pl.when(p > z if going_up else p < z)
            def _():
                pass_on(
                    going_up, with_sides(term(p * ny + y, wrest[j]), p, j), p * units + ny + j
                )

    def close_query():
        for d in range(ny):
            yy = (y + d) % ny
            b, slot = z * ny + yy, z * units + yy
            acc = term(b, wq[...])
            small = flat[b]

            def keep(acc, small):
                if d == 0:
                    q_out[...] = acc
                    flat_out[b] = small
                else:
                    last_out[d - 1] = acc.astype(BF16)
                    flat_last_out[d - 1] = small

            def lower():
                arrived(below.at[slot], below_got.at[slot])
                arrived(flat_below.at[b], fbelow_got.at[b])
                return below[slot].astype(F32), flat_below[b]

            def upper():
                arrived(above.at[slot], above_got.at[slot])
                arrived(flat_above.at[b], fabove_got.at[b])
                return above[slot].astype(F32), flat_above[b]

            @pl.when(z == 0)
            def _():
                more, less = upper()
                keep(acc + more, small + less)

            @pl.when(z == nz - 1)
            def _():
                more, less = lower()
                keep(acc + more, small + less)

            @pl.when(jnp.logical_and(z > 0, z < nz - 1))
            def _():
                more, less = lower()
                again, still = upper()
                keep(acc + more + again, small + less + still)

            if d:
                last(d).start()
                flat_last(d).start()

    lax.fori_loop(0, chunks, side_round, 0)
    close_at = early + lag * (nz - 1) + 1

    def step(n, carry):
        @pl.when(n == 1)
        def _():
            lax.fori_loop(chunks, (nz - 1) * chunks, side_round, 0)
            lax.fori_loop(0, chunks, side_own, 0)

        flow(True, n - lag * z)
        flow(False, n - lag * (nz - 1 - z))

        @pl.when(n == close_at)
        def _():
            close_query()

        return carry

    lax.fori_loop(0, max(total + lag * (nz - 1), close_at + 1), step, 0)

    def close_rest(j, carry):
        slot = z * units + ny + j
        acc = with_sides(term(me, wrest[j]), z, j)
        at = pl.ds(pl.multiple_of(j * width, width), width)

        @pl.when(z == 0)
        def _():
            arrived(above.at[slot], above_got.at[slot])
            rest_out[:, at] = acc + above[slot].astype(F32)

        @pl.when(z == nz - 1)
        def _():
            arrived(below.at[slot], below_got.at[slot])
            rest_out[:, at] = acc + below[slot].astype(F32)

        @pl.when(jnp.logical_and(z > 0, z < nz - 1))
        def _():
            arrived(below.at[slot], below_got.at[slot])
            arrived(above.at[slot], above_got.at[slot])
            rest_out[:, at] = acc + below[slot].astype(F32) + above[slot].astype(F32)

        return carry

    lax.fori_loop(0, chunks, close_rest, 0)
    small = flat_out[me]
    for d in range(1, ny):
        arrived(last_in.at[d - 1], last_got.at[d - 1])
        q_out[...] = q_out[...] + last_in[d - 1].astype(F32)
        arrived(flat_last_in.at[d - 1], flast_got.at[d - 1])
        small = small + flat_last_in[d - 1]
    spare = jnp.zeros((LANES - small.shape[0], rows), F32)
    gates_out[...] = jnp.concatenate([small, spare], axis=0).T

    for d in range(1, ny):
        last(d).wait_send()
        flat_last(d).wait_send()

    def drain_side(u, carry):
        for d in range(1, ny):
            side(d, u // chunks, u % chunks).wait_send()
        return carry

    lax.fori_loop(0, nz * chunks, drain_side, 0)

    def drain_line(slot, carry):
        p = slot // units

        @pl.when(p > z)
        def _():
            line(True, slot).wait_send()

        @pl.when(p < z)
        def _():
            line(False, slot).wait_send()

        return carry

    lax.fori_loop(0, nz * units, drain_line, 0)

    def drain_flat(b, carry):
        @pl.when(b // ny > z)
        def _():
            flat_line(True, b).wait_send()

        @pl.when(b // ny < z)
        def _():
            flat_line(False, b).wait_send()

        return carry

    lax.fori_loop(0, nz * ny, drain_flat, 0)


def gather_sums(tokens, gain, gate_rows, query, key, value, outgate, ny, nz):
    kv = ny * nz
    depth = tokens.shape[1]
    rows = tokens.shape[0] // kv
    width = query.shape[1]
    chunks = (key.shape[1] + value.shape[1] + outgate.shape[1]) // width
    units = ny + chunks
    small = gate_rows.shape[0] + 8
    others = max(ny - 1, 1)
    vmem = pl.BlockSpec(memory_space=pltpu.VMEM)
    anywhere = pl.BlockSpec(memory_space=pl.ANY)
    dma = pltpu.SemaphoreType.DMA
    unit = (rows, width)
    tiny = (small, rows)
    return pl.pallas_call(
        functools.partial(gather_sums_kernel, ny, nz, 2),
        out_shape=[
            jax.ShapeDtypeStruct(unit, F32),
            jax.ShapeDtypeStruct((rows, chunks * width), F32),
            jax.ShapeDtypeStruct((rows, LANES), F32),
        ],
        in_specs=[anywhere, vmem, vmem] + [anywhere] * 4,
        out_specs=[vmem] * 3,
        scratch_shapes=[
            pltpu.VMEM(tokens.shape, BF16),
            pltpu.VMEM(tokens.shape, BF16),
            pltpu.VMEM((depth, width), BF16),
            pltpu.VMEM((chunks, depth, width), BF16),
            pltpu.VMEM((kv,) + tiny, F32),
            pltpu.VMEM((others, nz * chunks) + unit, BF16),
            pltpu.VMEM((others, nz * chunks) + unit, BF16),
            pltpu.VMEM((nz * units,) + unit, BF16),
            pltpu.VMEM((nz * units,) + unit, BF16),
            pltpu.VMEM((nz * units,) + unit, BF16),
            pltpu.VMEM((others,) + unit, BF16),
            pltpu.VMEM((others,) + unit, BF16),
            pltpu.VMEM((kv,) + tiny, F32),
            pltpu.VMEM((kv,) + tiny, F32),
            pltpu.VMEM((kv,) + tiny, F32),
            pltpu.VMEM((others,) + tiny, F32),
            pltpu.VMEM((others,) + tiny, F32),
            dma((2 + chunks,)),
            dma((others, nz * chunks)),
            dma((others, nz * chunks)),
            dma((nz * units,)),
            dma((nz * units,)),
            dma((nz * units,)),
            dma((others,)),
            dma((others,)),
            dma((kv,)),
            dma((kv,)),
            dma((kv,)),
            dma((others,)),
            dma((others,)),
        ],
        compiler_params=pltpu.CompilerParams(collective_id=1, has_side_effects=True),
        cost_estimate=pl.CostEstimate(
            flops=2 * kv * rows * depth * width * (chunks + 1),
            bytes_accessed=2 * depth * width * (chunks + 1),
            transcendentals=0,
        ),
        name="gather_sums",
    )(tokens, gain, gate_rows, query, key, value, outgate)


def per_device(
    kv,
    tp,
    tokens,
    norm_gain,
    query_weight,
    key_weight,
    value_weight,
    outgate_weight,
    gate_weight,
    forget_bias,
    head_gain,
    output_weight,
    state_matrix,
    state_normal,
    state_stable,
    prior_keys,
    prior_values,
    prior_ingate,
    prior_forget,
    accepted,
    parents,
):
    ny = 1 << ((kv.bit_length() - 1) // 2)
    nz = kv // ny
    me = lax.axis_index("kv")
    mine = lax.axis_index("tp")
    z, y = me // ny, lax.rem(me, ny)
    heads = query_weight.shape[1] // DQK
    depth = tokens.shape[1]
    seqs = accepted.shape[0]
    rows = seqs * PROP

    own_gain = lax.dynamic_slice_in_dim(norm_gain, me * depth, depth, 0)[None, :]
    head_start = mine * heads
    picked = lax.dynamic_slice_in_dim(
        gate_weight.reshape(depth, 2, HEADS), head_start, heads, 2
    ).reshape(depth, 2 * heads)
    sq_lane = -(-2 * heads // 8) * 8
    gate_rows = jnp.pad(picked.T, ((0, sq_lane - 2 * heads), (0, 0)))
    query, rest, gates = gather_sums(
        tokens, own_gain, gate_rows, query_weight, key_weight, value_weight, outgate_weight, ny, nz
    )

    live = (jnp.arange(PROP, dtype=jnp.int32)[None, :] < accepted[:, None])[:, :, None]
    forget_live = jnp.where(live, prior_forget, 0.0)
    cumul = [forget_live[:, 0]]
    for p in range(1, PROP):
        cumul.append(cumul[-1] + forget_live[:, p])
    total = cumul[-1]
    cumul = jnp.stack(cumul, axis=1)
    weight_log = jnp.where(live, total[:, None, :] - cumul + prior_ingate, -jnp.inf)
    new_stable = jnp.maximum(total + state_stable, jnp.max(weight_log, axis=1))
    weights = jnp.exp(weight_log - new_stable[:, None, :])
    decay = jnp.exp(total + state_stable - new_stable)
    new_normal = decay[:, :, None] * state_normal + jnp.sum(
        weights[..., None] * prior_keys.astype(F32).reshape(seqs, PROP, heads, DQK), axis=1
    )
    weight_rows = jnp.pad(weights.reshape(rows, heads), ((0, 0), (0, LANES - heads)))
    new_matrix, low_matrix = commit_matrix(
        decay,
        state_matrix,
        prior_keys.reshape(rows, heads * DQK),
        prior_values.reshape(rows, heads * DV),
        weight_rows,
        4,
    )

    step_rows = 32
    group = step_rows // PROP
    table = ancestry(parents)
    spread = (
        table.reshape(seqs // group, group, PROP, 1, PROP)
        * jnp.eye(group, dtype=F32)[None, :, None, :, None]
    ).reshape(rows, step_rows)
    stable_rows = jnp.pad(
        jnp.repeat(new_stable, PROP, axis=0), ((0, 0), (heads, LANES - 2 * heads))
    )
    normal_rows = jnp.repeat(new_normal.reshape(seqs, heads * DQK), PROP, axis=0)
    bias = jnp.pad(
        lax.dynamic_slice_in_dim(forget_bias, head_start, heads, 0), (heads, LANES - 2 * heads)
    )[None, :]

    hidden = tree_read(
        query,
        rest,
        gates,
        sq_lane,
        low_matrix,
        spread,
        stable_rows,
        normal_rows,
        bias,
        head_gain[None, :],
        step_rows,
    )

    layer_out = spread_out(hidden, output_weight, ny, nz, tp)
    return (layer_out, new_matrix, new_normal, new_stable)


def solution(mesh):
    placed = (
        P(None, "kv"),
        P(),
        P("kv", "tp"),
        P("kv", "tp"),
        P("kv", "tp"),
        P("kv", "tp"),
        P("kv", None),
        P(),
        P("tp"),
        P("tp", "kv"),
        P("kv", "tp", None, None),
        P("kv", "tp", None),
        P("kv", "tp"),
        P("kv", None, "tp"),
        P("kv", None, "tp"),
        P("kv", None, "tp"),
        P("kv", None, "tp"),
        P("kv"),
        P("kv", None),
    )
    return jax.shard_map(
        functools.partial(per_device, mesh.shape["kv"], mesh.shape["tp"]),
        mesh=mesh,
        in_specs=placed,
        out_specs=(P("tp", "kv"), P("kv", "tp", None, None), P("kv", "tp", None), P("kv", "tp")),
        check_vma=False,
    )
```

profile of v0, /device:TPU:0, one launch (start us, length us, event | category | flops | bytes accessed | tf_op | source)
XLA Modules:
  0.0 150.4 jit_solution(13967203536804517741)
XLA Ops:
  0.7 0.7 iota_compare_fusion.8
  1.4 0.7 broadcast_select_fusion
  2.1 0.7 fusion.4
  2.8 0.1 copy.67
  2.9 0.1 copy.65
  3.0 0.8 copy.66
  3.8 0.6 subtract_exponential_fusion
  4.5 0.1 copy.69
  4.6 0.6 pad.12.w_ref
  5.2 1.7 %reshape.130.v_ref = bf16[128,1024]{1,0:T(8,128)(2,1)} reshape(bf16[32,4,1024]{2,1,0:T(4,128)(2,1)} %param.33) | data formatting | bytes 524288 | tf_op jit(solution)/shard_map/reshape | solution.py:828
  6.9 1.6 %reshape.129.k_ref = bf16[128,512]{1,0:T(8,128)(2,1)} reshape(bf16[32,4,512]{2,1,0:T(4,128)(2,1)} %param.32) | data formatting | bytes 262144 | tf_op jit(solution)/shard_map/reshape | solution.py:827
  8.5 16.8 %commit.1 = (f32[32,4,128,256]{3,2,1,0:T(8,128)}, bf16[32,4,128,256]{3,2,1,0:T(8,128)(2,1)}) custom-call(f32[32,4]{1,0:T(8,128)} %get-tuple-element.32.decay_ref, f32[32,4,128,256]{3,2,1,0:T(8,128)} %m_ref.1, bf16[128,512]{1,0:T(8,128)(2,1)} %reshape.129.k_ref, bf16[128,1024]{1,0:T(8,128)(2,1)} %reshape.130.v_ref, f32[128,128]{1,0:T(8,128)} %pad.12.w_ref), custom_call_target="tpu_custom_call" | custom-call | flops 67108864 | bytes 41943040 | tf_op jit(solution)/shard_map/commit/pallas_call | solution.py:64
  25.3 0.2 mul.50
  25.5 0.2 mul.51
  25.7 0.2 multiply_reduce_fusion
  25.9 0.1 multiply_add_fusion
  26.1 0.8 reshape.134.normal_ref
  26.9 0.7 pad.13.stable_ref
  27.7 0.1 reduce_sum.46
  28.0 0.1 copy.71
  28.1 0.1 copy.72
  28.2 0.1 copy.70
  28.3 0.1 broadcast_multiply_fusion
  28.4 0.3 mul.47
  28.7 0.7 copy.75.table_ref
  29.4 0.6 reshape.128
  30.0 1.3 dynamic_slice.9
  31.4 73.9 %gather_sums.1 = (f32[128,512]{1,0:T(8,128)}, f32[128,2560]{1,0:T(8,128)}, f32[128,128]{1,0:T(8,128)}) custom-call(bf16[1024,512]{1,0:T(8,128)(2,1)} %tok_hbm.1, f32[1,512]{1,0:T(1,128)} %bitcast.40, bf16[8,512]{1,0:T(8,128)(2,1)} %bitcast.38, bf16[512,512]{1,0:T(8,128)(2,1)} %q_hbm.1, bf16[512,512]{1,0:T(8,128)(2,1)} %k_hbm.1, bf16[512,1024]{1,0:T(8,128)(2,1)} %v_hbm.1, ...), custom_call_target="tpu_custom_call" | custom-call | flops 3221225472 | bytes 3145728 | tf_op jit(solution)/shard_map/gather_sums/pallas_call | solution.py:714
  105.4 0.6 pad_bitcast_fusion.bias_ref
  106.0 9.1 %tree_read.1.hid_ref = bf16[128,1024]{1,0:T(8,128)(2,1)} custom-call(f32[128,512]{1,0:T(8,128)} %get-tuple-element.9.q_ref, f32[128,2560]{1,0:T(8,128)} %get-tuple-element.10.rest_ref, f32[128,128]{1,0:T(8,128)} %get-tuple-element.11.gates_ref, bf16[32,4,128,256]{3,2,1,0:T(8,128)(2,1)} %get-tuple-element.12.m_ref, f32[128,32]{1,0:T(8,128)} %copy.75.table_ref, ...), custom_call_target="tpu_custom_call" | custom-call | flops 33554432 | bytes 8388608 | tf_op jit(solution)/shard_map/tree_read/pallas_call | solution.py:165
  115.1 33.6 %spread.1 = bf16[256,512]{1,0:T(8,128)(2,1)} custom-call(bf16[128,1024]{1,0:T(8,128)(2,1)} %tree_read.1.hid_ref, bf16[1024,512]{1,0:T(8,128)(2,1)} %w_ref.1), custom_call_target="tpu_custom_call" | custom-call | flops 1073741824 | bytes 1048576 | tf_op jit(solution)/shard_map/spread/pallas_call | solution.py:359
  148.8 1.7 %copy.84 = bf16[256,512]{1,0:T(8,128)(2,1)} copy(bf16[256,512]{1,0:T(8,128)(2,1)} %spread.1) | data formatting | bytes 524288
  (36 shorter events, 0.6 us)
Async XLA Ops:
  0.6 28.8 %copy-start = (bf16[512,32]{0,1:T(8,128)(2,1)S(1)}, bf16[512,32]{0,1:T(8,128)(2,1)}, u32[]{:S(2)}) copy-start(bf16[512,32]{0,1:T(8,128)(2,1)} %param.25) | copy-start | bytes 98308
  0.6 25.0 %copy-start.1 = (bf16[32,4,512]{2,1,0:T(4,128)(2,1)S(1)}, bf16[32,4,512]{2,1,0:T(4,128)(2,1)}, u32[]{:S(2)}) copy-start(bf16[32,4,512]{2,1,0:T(4,128)(2,1)} %param.32) | copy-start | bytes 393220
  0.7 25.3 %copy-start.4 = (f32[32,4,128]{2,1,0:T(4,128)S(1)}, f32[32,4,128]{2,1,0:T(4,128)}, u32[]{:S(2)}) copy-start(f32[32,4,128]{2,1,0:T(4,128)} %param.30) | copy-start | bytes 196612
  0.7 27.0 %copy-start.5 = (s32[32,4]{0,1:T(4,128)S(1)}, s32[32,4]{0,1:T(4,128)}, u32[]{:S(2)}) copy-start(s32[32,4]{0,1:T(4,128)} %param.37) | copy-start | bytes 1540
  4.4 21.6 %copy-start.3 = (f32[32,4]{1,0:T(8,128)S(1)}, f32[32,4]{1,0:T(8,128)}, u32[]{:S(2)}) copy-start(f32[32,4]{1,0:T(8,128)} %get-tuple-element.32.decay_ref) | copy-start | bytes 1540
  4.4 100.9 %copy-start.6 = (f32[32,4]{0,1:T(4,128)}, f32[32,4]{0,1:T(4,128)S(1)}, u32[]{:S(2)}) copy-start(f32[32,4]{0,1:T(4,128)S(1)} %copy.68) | copy-start | bytes 1540
  8.5 96.8 %copy-start.7 = (f32[16]{0:T(128)S(1)}, f32[16]{0:T(128)}, u32[]{:S(2)}) copy-start(f32[16]{0:T(128)} %param.26) | copy-start | bytes 196
  26.0 124.4 %copy-start.2 = (f32[32,4,128]{2,1,0:T(4,128)}, f32[32,4,128]{2,1,0:T(4,128)S(1)}, u32[]{:S(2)}) copy-start(f32[32,4,128]{2,1,0:T(4,128)S(1)} %multiply_add_fusion) | copy-start | bytes 196612
where the time goes:
time: 151 us; the launch traced here: 150 us
  Pallas kernels  133 us (88%)
  local copies, waits for them, and re-layouts  12.9 us (9%)
  other arithmetic  3.26 us (2%)
    pallas_call x1, Pallas kernels, gather_sums(): pl.pallas_call(functools.partial(gather_sums_kernel, ny, nz, 2), out_shap...  73.9 us
    pallas_call x1, Pallas kernels, spread_out(): pl.pallas_call(functools.partial(spread_kernel, ny, nz, tp, cuts), out_sh...  33.6 us
    pallas_call x1, Pallas kernels, commit_matrix(): pl.pallas_call(functools.partial(commit_kernel, seqs, heads), grid=(total...  16.8 us
    pallas_call x1, Pallas kernels, tree_read(): pl.pallas_call(functools.partial(read_kernel, heads, sq_lane), grid=(tota...  9.14 us

commit v1 on v0

v1 whole, which is shorter than its diff:
```python
import functools

import jax
import jax.numpy as jnp
from jax import lax
from jax.experimental import pallas as pl
from jax.experimental.pallas import tpu as pltpu
from jax.sharding import PartitionSpec as P

D = 4096
HEADS = 16
DQK = 128
DV = 256
PROP = 4
LANES = 128
NEG = -1e30
F32 = jnp.float32
BF16 = jnp.bfloat16
HP = lax.Precision.HIGHEST


def tree_kernel(
    q_ref, rest_ref, gates_ref, state_ref, mat, normal_ref, stable_ref, parent_ref, bias_ref,
    gain_ref, out_ref, mat_hbm, normal_out, stable_out, sem,
):
    mine = lax.axis_index("tp")
    rows = q_ref.shape[0]
    seqs, heads = mat.shape[:2]
    sq_lane = -(-2 * heads // 8) * 8
    stores = [pltpu.make_async_copy(mat.at[s], mat_hbm.at[s], sem.at[s]) for s in range(seqs)]
    for store in stores:
        store.start()
    stable_out[...] = stable_ref[...]

    def exact(a, b):
        return jnp.dot(a, b, precision=HP, preferred_element_type=F32)

    def iota(shape, axis):
        return lax.broadcasted_iota(jnp.int32, shape, axis)

    parents = parent_ref[...]
    current = iota((PROP, seqs), 0)
    tables = [(current == a).astype(F32) for a in range(PROP)]
    for repeat in range(PROP - 1):
        looked = jnp.zeros_like(current)
        for a in range(PROP):
            looked = looked + jnp.where(current == a, parents[a : a + 1], 0)
        current = jnp.where(current >= 0, looked, -1)
        tables = [t + (current == a).astype(F32) for a, t in enumerate(tables)]
    seq, at = iota((seqs, rows), 0), iota((seqs, rows), 1)
    packed = None
    for a, t in enumerate(tables):
        got = jnp.dot(
            t.astype(BF16), (at == seq * PROP + a).astype(F32).astype(BF16),
            preferred_element_type=F32,
        )
        packed = got if packed is None else packed + got
    spread = jnp.dot(
        (iota((rows, PROP), 0) % PROP == iota((rows, PROP), 1)).astype(F32).astype(BF16),
        packed.astype(BF16),
        preferred_element_type=F32,
    )
    same = iota((rows, rows), 0) // PROP == iota((rows, rows), 1) // PROP
    table = jnp.where(same, spread, 0.0)
    own = (iota((rows, seqs), 0) // PROP == iota((rows, seqs), 1)).astype(F32)

    gates = gates_ref[...]
    scale = lax.rsqrt(gates[:, sq_lane : sq_lane + 1] * (1.0 / D) + 1e-06)
    gates = scale * gates
    from_bias = (
        iota((HEADS, LANES), 0) + heads == iota((HEADS, LANES), 1) + mine * heads
    ).astype(F32)
    x = gates + exact(bias_ref[...], from_bias)
    logforget = jnp.minimum(x, 0.0) - jnp.log1p(jnp.exp(-jnp.abs(x)))
    path = exact(table, logforget)
    lifted = pltpu.roll(gates, heads, 1) - path
    flat = lifted.T
    stable = jnp.concatenate(
        [stable_ref[...], jnp.zeros((LANES - heads, seqs), F32)], axis=0
    )
    carried_all = path + pltpu.roll(
        lax.dot_general(
            own, stable, (((1,), (1,)), ((), ())), precision=HP, preferred_element_type=F32
        ),
        heads, 1,
    )
    key_scale = scale / jnp.sqrt(jnp.float32(DQK))
    at_value = heads * DQK
    at_gate = at_value + heads * DV
    for h in range(heads):
        normal = normal_ref[h]
        normal_out[:, h, :] = normal
        query = scale * q_ref[:, h * DQK : (h + 1) * DQK]
        value = scale * rest_ref[:, at_value + h * DV : at_value + (h + 1) * DV]
        key = key_scale * rest_ref[:, h * DQK : (h + 1) * DQK]
        outgate = scale * rest_ref[:, at_gate + h * DV : at_gate + (h + 1) * DV]
        dlog = path[:, heads + h : heads + h + 1] + flat[heads + h : heads + h + 1, :]
        dlog = jnp.where(table > 0.5, dlog, NEG)
        carried = carried_all[:, heads + h : heads + h + 1]
        top = jnp.maximum(carried, jnp.max(dlog, axis=1, keepdims=True))
        scores = lax.dot_general(
            query, key, (((1,), (1,)), ((), ())), precision=HP, preferred_element_type=F32
        ) * jnp.exp(dlog - top)
        factor = jnp.exp(carried - top)
        from_state = scale * state_ref[:, h * DV : (h + 1) * DV]
        numer = exact(scores, value) + factor * from_state
        denom = jnp.sum(scores, axis=1, keepdims=True) + factor * jnp.sum(
            query * exact(own, normal), axis=1, keepdims=True
        )
        read = numer / jnp.maximum(jnp.abs(denom), jnp.exp(-top))
        normer = lax.rsqrt(jnp.mean(read * read, axis=1, keepdims=True) + 1e-06)
        hidden = (
            read
            * normer
            * gain_ref[:, h * DV : (h + 1) * DV]
            * (1.0 / (1.0 + jnp.exp(-outgate)))
        )
        out_ref[:, h * DV : (h + 1) * DV] = hidden.astype(BF16)
    for store in stores:
        store.wait()


def tree_read(query, rest, gates, state, matrix, normal, stable, parents, bias, gain):
    rows = query.shape[0]
    seqs, heads = matrix.shape[:2]
    vmem = pl.BlockSpec(memory_space=pltpu.VMEM)
    return pl.pallas_call(
        tree_kernel,
        out_shape=[
            pltpu.VMEM((rows, heads * DV), BF16),
            jax.ShapeDtypeStruct(matrix.shape, F32),
            jax.ShapeDtypeStruct((seqs, heads, DQK), F32),
            jax.ShapeDtypeStruct((heads, seqs), F32),
        ],
        in_specs=[vmem] * 10,
        out_specs=[vmem, pl.BlockSpec(memory_space=pl.ANY), vmem, vmem],
        scratch_shapes=[pltpu.SemaphoreType.DMA((seqs,))],
        compiler_params=pltpu.CompilerParams(vmem_limit_bytes=16 << 20),
        cost_estimate=pl.CostEstimate(
            flops=8 * matrix.size, bytes_accessed=matrix.size * 4, transcendentals=0
        ),
        name="tree_read",
    )(query, rest, gates, state, matrix, normal, stable, parents, bias, gain)


def two_terms(full):
    lead = full.astype(BF16)
    return lead, (full - lead.astype(F32)).astype(BF16)


def fold(full, fine):
    return (full * full * full * jnp.abs(full) if fine else full).astype(BF16)


def unfold(sent, fine):
    full = sent.astype(F32)
    if not fine:
        return full
    root = jnp.sqrt(jnp.sqrt(jnp.abs(full)))
    return jnp.where(full < 0.0, -root, root)


def by_kind(j, act):
    if isinstance(j, int):
        act(j == 0)
    else:
        pl.when(j == 0)(lambda: act(True))
        pl.when(j > 0)(lambda: act(False))


def remote(src, dst, send_sem, recv_sem, kv_index, tp_index):
    return pltpu.make_async_remote_copy(
        src_ref=src,
        dst_ref=dst,
        send_sem=send_sem,
        recv_sem=recv_sem,
        device_id=(kv_index, tp_index),
        device_id_type=pl.DeviceIdType.MESH,
    )


def greet(others):
    barrier = pltpu.get_barrier_semaphore()
    for other in others:
        pl.semaphore_signal(
            barrier, inc=1, device_id=other, device_id_type=pl.DeviceIdType.MESH
        )
    pl.semaphore_wait(barrier, len(others))


def spread_kernel(
    ny, nz, tp, cuts, hid_ref, w_ref, out_ref, held, parts, landed, total,
    up_sem, down_sem, side_sem, got_sem, part_sem, land_sem,
):
    me = lax.axis_index("kv")
    mine = lax.axis_index("tp")
    z, y = me // ny, lax.rem(me, ny)
    kv = ny * nz
    per = kv // tp
    rows = hid_ref.shape[0]
    piece = rows // cuts
    greet(
        [((z + d) % nz * ny + y, mine) for d in sorted({1 % nz, nz - 1}) if d]
        + [(z * ny + (y + d) % ny, mine) for d in range(1, ny)]
        + [(me, (mine + d) % tp) for d in range(1, tp)]
    )

    def slab(b, c):
        return held.at[b, pl.ds(c * piece, piece)]

    def source(s, b, c):
        return hid_ref.at[pl.ds(c * piece, piece)] if s == 0 else slab(b, c)

    def up(s, b, c):
        return remote(source(s, b, c), slab(b, c), up_sem.at[s, c], got_sem.at[b, c], me + ny, mine)

    def down(s, b, c):
        return remote(source(s, b, c), slab(b, c), down_sem.at[s, c], got_sem.at[b, c], me - ny, mine)

    def side(s, b, c, d, way):
        return remote(
            source(s, b, c), slab(b, c), side_sem.at[way, s, d - 1, c], got_sem.at[b, c],
            z * ny + (y + d) % ny, mine,
        )

    def arrive(b, c):
        return remote(slab(b, c), slab(b, c), part_sem.at[b], got_sem.at[b, c], me, mine)

    def product(s, b):
        value = hid_ref[...] if s == 0 else held[b]
        got = jnp.dot(value, w_ref[...], preferred_element_type=F32)
        owner = b // per
        slot = b % per

        @pl.when(owner == mine)
        def _():
            total[slot] = got

        @pl.when(owner != mine)
        def _():
            parts[b] = got.astype(BF16)

    pending = []

    def hand_on():
        for there, b in pending:
            @pl.when(jnp.logical_and(there, b // per != mine))
            def _():
                hand(b).start()
        pending.clear()

    def hand(b):
        owner = b // per
        slot = ((mine + tp - owner) % tp + tp - 1) % tp * per + b % per
        return remote(parts.at[b], landed.at[slot], part_sem.at[b], land_sem.at[slot], me, owner)

    for c in range(cuts):
        @pl.when(z < nz - 1)
        def _():
            up(0, me, c).start()

        @pl.when(z > 0)
        def _():
            down(0, me, c).start()

        for d in range(1, ny):
            side(0, me, c, d, 0).start()
    product(0, me)
    pending.append((z >= 0, me))

    def from_side(s, way, there):
        base = (z - s + nz) % nz * ny if way == 0 else (z + s) % nz * ny
        for d in range(1, ny):
            b = base + (y + d) % ny

            @pl.when(there)
            def _():
                for c in range(cuts):
                    arrive(b, c).wait_recv()
                product(1, b)

            hand_on()
            pending.append((there, b))

    def ways(s):
        return [(0, z - s >= 0)] if s == 0 else [(0, z - s >= 0), (1, z + s < nz)]

    for s in range(1, nz):
        for way, there in ways(s):
            b = ((z - s + nz) % nz if way == 0 else (z + s) % nz) * ny + y

            @pl.when(there)
            def _():
                for c in range(cuts):
                    arrive(b, c).wait_recv()
                    if s < nz - 1:
                        if way == 0:
                            @pl.when(z < nz - 1)
                            def _():
                                up(s, b, c).start()
                        else:
                            @pl.when(z > 0)
                            def _():
                                down(s, b, c).start()
                    for d in range(1, ny):
                        side(s, b, c, d, way).start()
                product(s, b)

            hand_on()
            pending.append((there, b))

        for way, there in ways(s - 1):
            from_side(s - 1, way, there)

    for way, there in ways(nz - 1):
        from_side(nz - 1, way, there)
    hand_on()

    for slot in range(per):
        acc = total[slot]
        for d in range(1, tp):
            at = (d - 1) * per + slot
            remote(landed.at[at], landed.at[at], part_sem.at[0], land_sem.at[at], me, mine).wait_recv()
            acc = acc + landed[at].astype(F32)
        out_ref[slot * rows : (slot + 1) * rows] = acc.astype(BF16)

    for s in range(nz):
        for way, there in ways(s):
            b = ((z - s + nz) % nz if way == 0 else (z + s) % nz) * ny + y

            @pl.when(there)
            def _():
                for c in range(cuts):
                    if s < nz - 1:
                        if way == 0:
                            @pl.when(z < nz - 1)
                            def _():
                                up(s, b, c).wait_send()
                        if way == 1 or s == 0:
                            @pl.when(z > 0)
                            def _():
                                down(s, b, c).wait_send()
                    for d in range(1, ny):
                        side(s, b, c, d, way).wait_send()
    for b in range(kv):
        @pl.when(b // per != mine)
        def _():
            hand(b).wait_send()


def spread_out(hidden, weight, ny, nz, tp):
    rows, width = hidden.shape
    cols = weight.shape[1]
    kv = ny * nz
    per = kv // tp
    cuts = 2
    vmem = pl.BlockSpec(memory_space=pltpu.VMEM)
    dma = pltpu.SemaphoreType.DMA
    return pl.pallas_call(
        functools.partial(spread_kernel, ny, nz, tp, cuts),
        out_shape=jax.ShapeDtypeStruct((per * rows, cols), BF16),
        in_specs=[vmem, vmem],
        out_specs=vmem,
        scratch_shapes=[
            pltpu.VMEM((kv, rows, width), BF16),
            pltpu.VMEM((kv, rows, cols), BF16),
            pltpu.VMEM(((tp - 1) * per, rows, cols), BF16),
            pltpu.VMEM((per, rows, cols), F32),
            dma((nz, cuts)),
            dma((nz, cuts)),
            dma((2, nz, max(ny - 1, 1), cuts)),
            dma((kv, cuts)),
            dma((kv,)),
            dma(((tp - 1) * per,)),
        ],
        compiler_params=pltpu.CompilerParams(
            collective_id=0, has_side_effects=True, vmem_limit_bytes=16 << 20
        ),
        cost_estimate=pl.CostEstimate(
            flops=2 * kv * rows * width * cols, bytes_accessed=8 * rows * width, transcendentals=0
        ),
        name="spread",
    )(hidden, weight)


def gather_sums_kernel(
    ny, nz, lag, tok_hbm, gain_ref, gate_ref, q_hbm, k_hbm, v_hbm, o_hbm, state_hbm,
    pk_ref, pv_ref, pin_ref, pfo_ref, stable_ref, count_ref, normal_ref,
    q_out, rest_out, gates_out, state_out, mat, normal_out, stable_out,
    tok, normed, wq, wrest, flat,
    side_out, side_in, line_out, below, above, last_out, last_in,
    flat_out, flat_below, flat_above, flat_last_out, flat_last_in,
    wide, kt, vw, decay, work,
    load_sem, side_sem, side_got, line_sem, below_got, above_got, last_sem, last_got,
    fline_sem, fbelow_got, fabove_got, flast_sem, flast_got, state_sem,
):
    me = lax.axis_index("kv")
    mine = lax.axis_index("tp")
    z, y = me // ny, lax.rem(me, ny)
    rows = q_out.shape[0]
    width = wq.shape[1]
    chunks = wrest.shape[0]
    units = ny + chunks
    seqs, heads = mat.shape[:2]
    depth = tok.shape[1]

    loads = [
        pltpu.make_async_copy(tok_hbm, tok, load_sem.at[0]),
        pltpu.make_async_copy(q_hbm, wq, load_sem.at[1]),
    ]
    for n, (w, at) in enumerate(
        [(w, at) for w in (k_hbm, v_hbm, o_hbm) for at in range(0, w.shape[1], width)]
    ):
        loads.append(
            pltpu.make_async_copy(w.at[:, pl.ds(at, width)], wrest.at[n], load_sem.at[2 + n])
        )
    for load in loads:
        load.start()

    def state_load(s):
        return pltpu.make_async_copy(state_hbm.at[s], mat.at[s], state_sem.at[s])

    greet(
        [((z + d) % nz * ny + y, mine) for d in sorted({1 % nz, nz - 1}) if d]
        + [(z * ny + (y + d) % ny, mine) for d in range(1, ny)]
    )
    loads[0].wait()
    gain = gain_ref[:, pl.ds(pl.multiple_of(me * depth, LANES), depth)]

    def prepare(n, carry):
        at = pl.ds(pl.multiple_of(n * rows, rows), rows)
        normed[at, :] = (tok[at, :].astype(F32) * gain).astype(BF16)
        return carry

    lax.fori_loop(0, ny * nz, prepare, 0)
    for load in loads[1:]:
        load.wait()

    small = flat.shape[1] - 8
    row = lax.broadcasted_iota(jnp.int32, (small, 2 * HEADS), 0)
    col = lax.broadcasted_iota(jnp.int32, (small, 2 * HEADS), 1)
    want = jnp.where(row < heads, row, HEADS - heads + row) + mine * heads
    picked = jnp.where(jnp.logical_and(row < 2 * heads, col == want), 1.0, 0.0).astype(BF16)
    gate_rows = jnp.dot(picked, gate_ref[...], preferred_element_type=F32).astype(BF16)

    def flats(n, carry):
        at = pl.ds(pl.multiple_of(n * rows, rows), rows)
        x = tok[at, :].astype(F32)
        full = x * x
        lead = full.astype(BF16)
        rest = (full - lead.astype(F32)).astype(BF16)
        ones = jnp.ones((8, depth), BF16)

        def across(a, b):
            return lax.dot_general(a, b, (((1,), (1,)), ((), ())), preferred_element_type=F32)

        flat[n] = jnp.concatenate(
            [across(gate_rows, normed[at, :]), across(ones, lead) + across(ones, rest)], axis=0
        )
        return carry

    def term(block, w):
        at = pl.ds(pl.multiple_of(block * rows, rows), rows)
        return jnp.dot(normed[at, :], w, preferred_element_type=F32)

    def side(d, p, j):
        u = p * chunks + j
        return remote(
            side_out.at[d - 1, u], side_in.at[ny - d - 1, u], side_sem.at[d - 1, u],
            side_got.at[ny - d - 1, u], z * ny + (y + d) % ny, mine,
        )

    def line(going_up, slot):
        got, sem, far = (below, below_got, me + ny) if going_up else (above, above_got, me - ny)
        return remote(line_out.at[slot], got.at[slot], line_sem.at[slot], sem.at[slot], far, mine)

    def flat_line(going_up, b):
        got, sem, far = (
            (flat_below, fbelow_got, me + ny) if going_up else (flat_above, fabove_got, me - ny)
        )
        return remote(flat_out.at[b], got.at[b], fline_sem.at[b], sem.at[b], far, mine)

    def last(d):
        return remote(
            last_out.at[d - 1], last_in.at[ny - d - 1], last_sem.at[d - 1],
            last_got.at[ny - d - 1], z * ny + (y + d) % ny, mine,
        )

    def flat_last(d):
        return remote(
            flat_last_out.at[d - 1], flat_last_in.at[ny - d - 1], flast_sem.at[d - 1],
            flast_got.at[ny - d - 1], z * ny + (y + d) % ny, mine,
        )

    def arrived(ref, sem):
        remote(ref, ref, load_sem.at[0], sem, me, mine).wait_recv()

    def fill_side(p, j):
        for d in range(1, ny):
            work[...] = term(p * ny + (y + d) % ny, wrest[j])

            def put(fine):
                side_out[d - 1, p * chunks + j] = fold(work[...], fine)

            by_kind(j, put)

    def start_side(p, j):
        for d in range(1, ny):
            side(d, p, j).start()

    def each_side(n, act):
        i, j = n // chunks, n % chunks

        @pl.when(jnp.logical_and(i < nz - 1, nz - 1 - i > z))
        def _():
            act(nz - 1 - i, j)

        @pl.when(i < z)
        def _():
            act(i, j)

        @pl.when(i == nz - 1)
        def _():
            act(z, j)

    def side_round(n, carry):
        each_side(n, fill_side)

        @pl.when(n > 0)
        def _():
            each_side(n - 1, start_side)

        return carry

    def add(ref, at, sem, j):
        arrived(ref.at[at], sem.at[at])

        def more(fine):
            work[...] = work[...] + unfold(ref[at], fine)

        by_kind(j, more)

    def add_sides(p, j):
        for d in range(1, ny):
            add(side_in, (d - 1, p * chunks + j), side_got, j)

    def pass_on(going_up, slot, j):
        got, sem = (below, below_got) if going_up else (above, above_got)

        @pl.when(z > 0 if going_up else z < nz - 1)
        def _():
            add(got, slot, sem, j)

        def put(fine):
            line_out[slot] = fold(work[...], fine)

        by_kind(j, put)

    def pass_flat(going_up, b):
        got, sem = (flat_below, fbelow_got) if going_up else (flat_above, fabove_got)
        first = z == 0 if going_up else z == nz - 1

        @pl.when(first)
        def _():
            flat_out[b] = flat[b]

        @pl.when(jnp.logical_not(first))
        def _():
            arrived(got.at[b], sem.at[b])
            flat_out[b] = flat[b] + got[b]

    early = (nz - 1) * ny
    total = early + (nz - 1) * chunks

    def plane_of(going_up, i):
        return nz - 1 - i if going_up else i

    def flow(going_up, n, send):
        @pl.when(jnp.logical_and(n >= 0, n < early))
        def _():
            p = plane_of(going_up, n // ny)

            @pl.when(p > z if going_up else p < z)
            def _():
                b = p * ny + n % ny
                if send:
                    flat_line(going_up, b).start()
                    line(going_up, p * units + n % ny).start()
                else:
                    pass_flat(going_up, b)
                    work[...] = term(b, wq[...])
                    pass_on(going_up, p * units + n % ny, 0)

        @pl.when(jnp.logical_and(n >= early, n < total))
        def _():
            p = plane_of(going_up, (n - early) // chunks)
            j = (n - early) % chunks

            @pl.when(p > z if going_up else p < z)
            def _():
                slot = p * units + ny + j
                if send:
                    line(going_up, slot).start()
                else:
                    work[...] = term(p * ny + y, wrest[j])
                    add_sides(p, j)
                    pass_on(going_up, slot, j)

    def close_query():
        for d in range(ny):
            yy = (y + d) % ny
            b, slot = z * ny + yy, z * units + yy
            acc = term(b, wq[...])
            small = flat[b]

            def keep(acc, small):
                if d == 0:
                    q_out[...] = acc
                    flat_out[b] = small
                else:
                    last_out[d - 1] = fold(acc, True)
                    flat_last_out[d - 1] = small

            def lower():
                arrived(below.at[slot], below_got.at[slot])
                arrived(flat_below.at[b], fbelow_got.at[b])
                return unfold(below[slot], True), flat_below[b]

            def upper():
                arrived(above.at[slot], above_got.at[slot])
                arrived(flat_above.at[b], fabove_got.at[b])
                return unfold(above[slot], True), flat_above[b]

            @pl.when(z == 0)
            def _():
                more, less = upper()
                keep(acc + more, small + less)

            @pl.when(z == nz - 1)
            def _():
                more, less = lower()
                keep(acc + more, small + less)

            @pl.when(jnp.logical_and(z > 0, z < nz - 1))
            def _():
                more, less = lower()
                again, still = upper()
                keep(acc + more + again, small + less + still)


    def exact(a, b):
        return jnp.dot(a, b, precision=HP, preferred_element_type=F32)

    def prepare_commit():
        run = None
        sums, lives = [], []
        for p in range(PROP):
            live = count_ref[...] > p
            here = jnp.where(live, pfo_ref[p], 0.0)
            run = here if run is None else run + here
            sums.append(run)
            lives.append(live)
        logs = [
            jnp.where(live, run - part + pin_ref[p], NEG)
            for p, (live, part) in enumerate(zip(lives, sums))
        ]
        carried = run + stable_ref[...]
        top = carried
        for log in logs:
            top = jnp.maximum(top, log)
        stable_out[...] = top
        seq = lax.broadcasted_iota(jnp.int32, (seqs, rows), 0)
        at = lax.broadcasted_iota(jnp.int32, (seqs, rows), 1)
        flat_weights = None
        for p, log in enumerate(logs):
            got = exact(jnp.exp(log - top), (at == seq * PROP + p).astype(F32))
            flat_weights = got if flat_weights is None else flat_weights + got
        spare = jnp.zeros((LANES - heads, rows), F32)
        weights = jnp.concatenate([flat_weights, spare], axis=0).T
        lanes = (
            lax.broadcasted_iota(jnp.int32, (seqs, LANES), 0)
            == lax.broadcasted_iota(jnp.int32, (seqs, LANES), 1)
        ).astype(F32)
        flat_decay = jnp.concatenate(
            [exact(jnp.exp(carried - top), lanes), jnp.zeros((LANES - heads, LANES), F32)], axis=0
        ).T

        pair = 8 // PROP

        def gather_keys(i, carry):
            to = pl.ds(pl.multiple_of(i * 8, 8), 8)
            got = [pk_ref[i * pair + n].astype(F32) for n in range(pair)]
            wide[to, : heads * DQK] = jnp.concatenate(got, axis=0)
            return carry

        lax.fori_loop(0, seqs // pair, gather_keys, 0)
        for h in range(heads):
            keys = wide[:, h * DQK : (h + 1) * DQK]
            kt[h] = keys.T
            mine_only = jnp.where(at // PROP == seq, flat_weights[h : h + 1], 0.0)
            fade = jnp.broadcast_to(flat_decay[:seqs, h : h + 1], (seqs, DV))
            decay[h] = fade
            normal_out[h] = fade[:, :DQK] * normal_ref[:, h, :] + exact(mine_only, keys)

        def gather_values(i, carry):
            to = pl.ds(pl.multiple_of(i * 8, 8), 8)
            got = [pv_ref[i * pair + n].astype(F32) for n in range(pair)]
            wide[to, :] = jnp.concatenate(got, axis=0)
            return carry

        lax.fori_loop(0, seqs // pair, gather_values, 0)
        for h in range(heads):
            at_h = slice(h * DV, (h + 1) * DV)
            lead, rest = two_terms(wide[:, at_h] * weights[:, h : h + 1])
            vw[:rows, at_h] = lead
            vw[rows:, at_h] = rest

    def commit(s):
        state_load(s).wait()
        own = lax.broadcasted_iota(jnp.int32, (DQK, rows), 1) // PROP == s
        for h in range(heads):
            lhs = jnp.where(own, kt[h], 0.0).astype(BF16)
            lhs = jnp.concatenate([lhs, lhs], axis=1)
            added = jnp.dot(lhs, vw[:, h * DV : (h + 1) * DV], preferred_element_type=F32)
            mat[s, h] = decay[h, pl.ds(s, 1), :] * mat[s, h] + added

    def finish_query():
        for d in range(1, ny):
            arrived(last_in.at[d - 1], last_got.at[d - 1])
            q_out[...] = q_out[...] + unfold(last_in[d - 1], True)

    def state_product(g):
        at = pl.ds(pl.multiple_of(g * 16, 16), 16)
        row16 = lax.broadcasted_iota(jnp.int32, (16, 1), 0) // PROP
        for h in range(heads):
            part, less = two_terms(q_out[at, h * DQK : (h + 1) * DQK])
            both = jnp.concatenate([part, less], axis=0)
            got = None
            for n in range(16 // PROP):
                lead, rest = two_terms(mat[g * (16 // PROP) + n, h])
                res = jnp.dot(both, lead, preferred_element_type=F32)
                res = res[:16] + res[16:] + jnp.dot(part, rest, preferred_element_type=F32)
                got = res if got is None else jnp.where(row16 == n, res, got)
            state_out[at, h * DV : (h + 1) * DV] = got

    lax.fori_loop(0, chunks + 1, side_round, 0)
    lax.fori_loop(0, ny * nz, flats, 0)
    close_at = early + lag * (nz - 1) + 1
    groups = rows // 16
    product_at = max(close_at + 2, 2 + seqs // 2)

    def step(n, carry):
        up_at, down_at = n - lag * z, n - lag * (nz - 1 - z)
        flow(True, up_at, False)
        flow(False, down_at, False)

        @pl.when(n == close_at)
        def _():
            close_query()

        @pl.when(jnp.logical_and(n >= 2, n < 2 + seqs // 2))
        def _():
            commit(2 * (n - 2))

        @pl.when(n == product_at)
        def _():
            finish_query()

        flow(True, up_at, True)
        flow(False, down_at, True)

        @pl.when(n == close_at)
        def _():
            for d in range(1, ny):
                last(d).start()
                flat_last(d).start()

        @pl.when(n == 1)
        def _():
            lax.fori_loop(chunks + 1, nz * chunks, side_round, 0)
            each_side(nz * chunks - 1, start_side)
            for s in range(seqs):
                state_load(s).start()
            prepare_commit()

        @pl.when(jnp.logical_and(n >= 2, n < 2 + seqs // 2))
        def _():
            commit(2 * (n - 2) + 1)

        @pl.when(jnp.logical_and(n >= product_at, n < product_at + groups))
        def _():
            state_product(n - product_at)

        return carry

    lax.fori_loop(0, max(total + lag * (nz - 1), product_at + groups), step, 0)

    def close_rest(j, carry):
        slot = z * units + ny + j
        work[...] = term(me, wrest[j])
        add_sides(z, j)

        @pl.when(z > 0)
        def _():
            add(below, slot, below_got, j)

        @pl.when(z < nz - 1)
        def _():
            add(above, slot, above_got, j)

        at = pl.ds(pl.multiple_of(j * width, width), width)
        rest_out[:, at] = work[...]
        return carry

    lax.fori_loop(0, chunks, close_rest, 0)
    small = flat_out[me]
    for d in range(1, ny):
        arrived(flat_last_in.at[d - 1], flast_got.at[d - 1])
        small = small + flat_last_in[d - 1]
    spare = jnp.zeros((LANES - small.shape[0], rows), F32)
    gates_out[...] = jnp.concatenate([small, spare], axis=0).T

    for d in range(1, ny):
        last(d).wait_send()
        flat_last(d).wait_send()

    def drain_side(u, carry):
        for d in range(1, ny):
            side(d, u // chunks, u % chunks).wait_send()
        return carry

    lax.fori_loop(0, nz * chunks, drain_side, 0)

    def drain_line(slot, carry):
        p = slot // units

        @pl.when(p > z)
        def _():
            line(True, slot).wait_send()

        @pl.when(p < z)
        def _():
            line(False, slot).wait_send()

        return carry

    lax.fori_loop(0, nz * units, drain_line, 0)

    def drain_flat(b, carry):
        @pl.when(b // ny > z)
        def _():
            flat_line(True, b).wait_send()

        @pl.when(b // ny < z)
        def _():
            flat_line(False, b).wait_send()

        return carry

    lax.fori_loop(0, nz * ny, drain_flat, 0)


def gather_sums(
    tokens, gain, gates, query, key, value, outgate, state, prior_keys, prior_values,
    ingate, forget, stable, count, normal, ny, nz,
):
    kv = ny * nz
    depth = tokens.shape[1]
    rows = tokens.shape[0] // kv
    width = query.shape[1]
    chunks = (key.shape[1] + value.shape[1] + outgate.shape[1]) // width
    units = ny + chunks
    seqs, heads = state.shape[:2]
    small = -(-2 * heads // 8) * 8 + 8
    others = max(ny - 1, 1)
    vmem = pl.BlockSpec(memory_space=pltpu.VMEM)
    anywhere = pl.BlockSpec(memory_space=pl.ANY)
    dma = pltpu.SemaphoreType.DMA
    unit = (rows, width)
    tiny = (small, rows)
    return pl.pallas_call(
        functools.partial(gather_sums_kernel, ny, nz, 2),
        out_shape=[
            pltpu.VMEM(unit, F32),
            pltpu.VMEM((rows, chunks * width), F32),
            pltpu.VMEM((rows, LANES), F32),
            pltpu.VMEM((rows, heads * DV), F32),
            pltpu.VMEM(state.shape, F32),
            pltpu.VMEM((heads, seqs, DQK), F32),
            pltpu.VMEM((heads, seqs), F32),
        ],
        in_specs=[anywhere, vmem, vmem] + [anywhere] * 5 + [vmem] * 7,
        out_specs=[vmem] * 7,
        scratch_shapes=[
            pltpu.VMEM(tokens.shape, BF16),
            pltpu.VMEM(tokens.shape, BF16),
            pltpu.VMEM((depth, width), BF16),
            pltpu.VMEM((chunks, depth, width), BF16),
            pltpu.VMEM((kv,) + tiny, F32),
            pltpu.VMEM((others, nz * chunks) + unit, BF16),
            pltpu.VMEM((others, nz * chunks) + unit, BF16),
            pltpu.VMEM((nz * units,) + unit, BF16),
            pltpu.VMEM((nz * units,) + unit, BF16),
            pltpu.VMEM((nz * units,) + unit, BF16),
            pltpu.VMEM((others,) + unit, BF16),
            pltpu.VMEM((others,) + unit, BF16),
            pltpu.VMEM((kv,) + tiny, F32),
            pltpu.VMEM((kv,) + tiny, F32),
            pltpu.VMEM((kv,) + tiny, F32),
            pltpu.VMEM((others,) + tiny, F32),
            pltpu.VMEM((others,) + tiny, F32),
            pltpu.VMEM((rows, heads * DV), F32),
            pltpu.VMEM((heads, DQK, rows), F32),
            pltpu.VMEM((2 * rows, heads * DV), BF16),
            pltpu.VMEM((heads, seqs, DV), F32),
            pltpu.VMEM(unit, F32),
            dma((2 + chunks,)),
            dma((others, nz * chunks)),
            dma((others, nz * chunks)),
            dma((nz * units,)),
            dma((nz * units,)),
            dma((nz * units,)),
            dma((others,)),
            dma((others,)),
            dma((kv,)),
            dma((kv,)),
            dma((kv,)),
            dma((others,)),
            dma((others,)),
            dma((seqs,)),
        ],
        compiler_params=pltpu.CompilerParams(
            collective_id=1, has_side_effects=True, vmem_limit_bytes=36 << 20
        ),
        cost_estimate=pl.CostEstimate(
            flops=2 * kv * rows * depth * width * (chunks + 1),
            bytes_accessed=2 * depth * width * (chunks + 1) + 4 * state.size,
            transcendentals=0,
        ),
        name="gather_sums",
    )(
        tokens, gain, gates, query, key, value, outgate, state, prior_keys, prior_values,
        ingate, forget, stable, count, normal,
    )


def per_device(
    kv,
    tp,
    tokens,
    norm_gain,
    query_weight,
    key_weight,
    value_weight,
    outgate_weight,
    gate_weight,
    forget_bias,
    head_gain,
    output_weight,
    state_matrix,
    state_normal,
    state_stable,
    prior_keys,
    prior_values,
    prior_ingate,
    prior_forget,
    accepted,
    parents,
):
    ny = 1 << ((kv.bit_length() - 1) // 2)
    nz = kv // ny
    query, rest, gates, state, matrix, normal, stable = gather_sums(
        tokens,
        norm_gain[None, :],
        gate_weight.T,
        query_weight,
        key_weight,
        value_weight,
        outgate_weight,
        state_matrix,
        prior_keys,
        prior_values,
        prior_ingate.transpose(1, 2, 0),
        prior_forget.transpose(1, 2, 0),
        state_stable.T,
        accepted[None, :],
        state_normal,
        ny,
        nz,
    )
    hidden, new_matrix, new_normal, new_stable = tree_read(
        query,
        rest,
        gates,
        state,
        matrix,
        normal,
        stable,
        parents.T,
        forget_bias[None, :],
        head_gain[None, :],
    )
    layer_out = spread_out(hidden, output_weight, ny, nz, tp)
    return (layer_out, new_matrix, new_normal, new_stable.T)


def solution(mesh):
    placed = (
        P(None, "kv"),
        P(),
        P("kv", "tp"),
        P("kv", "tp"),
        P("kv", "tp"),
        P("kv", "tp"),
        P("kv", None),
        P(),
        P("tp"),
        P("tp", "kv"),
        P("kv", "tp", None, None),
        P("kv", "tp", None),
        P("kv", "tp"),
        P("kv", None, "tp"),
        P("kv", None, "tp"),
        P("kv", None, "tp"),
        P("kv", None, "tp"),
        P("kv"),
        P("kv", None),
    )
    return jax.shard_map(
        functools.partial(per_device, mesh.shape["kv"], mesh.shape["tp"]),
        mesh=mesh,
        in_specs=placed,
        out_specs=(P("tp", "kv"), P("kv", "tp", None, None), P("kv", "tp", None), P("kv", "tp")),
        check_vma=False,
    )
```

time: 151 us -> 119 us (0.79)
  Pallas kernels: 133 us -> 117 us
  local copies, waits for them, and re-layouts: 12.9 us -> 0.72 us
  other arithmetic: 3.26 us -> 0 us
    pallas_call x2 -> x1, Pallas kernels: 25.9 us -> 8.62 us  [tree_read(): pl.pallas_call(tree_kernel, out_shape=[pltpu.VMEM((rows, heads * DV), BF1...]
    reshape x4 -> x0, local copies, waits for them, and re-layouts: 4.71 us -> none  [the longest x1 1.72 us: per_device(): prior_values.reshape(rows, heads * DV)]
    pallas_call x1, Pallas kernels: 73.9 us -> 78 us  [gather_sums(): pl.pallas_call(functools.partial(gather_sums_kernel, ny, nz, 2), out_shap...]
    pallas_call x1, Pallas kernels: 33.6 us -> 30.7 us  [spread_out(): pl.pallas_call(functools.partial(spread_kernel, ny, nz, tp, cuts), out_sh...]
    unnamed x20 -> x9, local copies, waits for them, and re-layouts: 2.48 us -> 0.72 us
where the time goes in v1:
time: 119 us
  Pallas kernels  117 us (98%)
    pallas_call x1, Pallas kernels, gather_sums(): pl.pallas_call(functools.partial(gather_sums_kernel, ny, nz, 2), out_shap...  78 us
    pallas_call x1, Pallas kernels, spread_out(): pl.pallas_call(functools.partial(spread_kernel, ny, nz, tp, cuts), out_sh...  30.7 us
    pallas_call x1, Pallas kernels, tree_read(): pl.pallas_call(tree_kernel, out_shape=[pltpu.VMEM((rows, heads * DV), BF1...  8.62 us

profile of v1, /device:TPU:0, one launch (start us, length us, event | category | flops | bytes accessed | tf_op | source)
XLA Modules:
  0.0 118.8 jit_solution(17982153173948424356)
XLA Ops:
  0.6 0.0 copy-start.1
  0.6 0.0 copy-start
  0.7 0.0 copy-start.2
  0.7 0.0 copy-start.3
  0.7 78.0 %gather_sums.1 = (f32[128,512]{1,0:T(8,128)S(1)}, f32[128,2560]{1,0:T(8,128)S(1)}, f32[128,128]{1,0:T(8,128)S(1)}, f32[128,1024]{1,0:T(8,128)S(1)}, f32[32,4,128...) custom-call(bf16[1024,512]{1,0:T(8,128)(2,1)} %tok_hbm.1, f32[1,4096]{1,0:T(1,128)} %bitcast.14, ...), custom_call_target="tpu_custom_call" | custom-call | flops 3221225472 | bytes 19922944 | tf_op jit(solution)/shard_map/gather_sums/pallas_call | solution.py:881
  78.7 0.0 copy-done.1
  78.7 0.0 copy-done
  78.7 0.0 copy-done.2
  78.7 8.6 %tree_read.1 = (bf16[128,1024]{1,0:T(8,128)(2,1)S(1)}, f32[32,4,128,256]{3,2,1,0:T(8,128)}, f32[32,4,128]{2,1,0:T(4,128)}, f32[4,32]{1,0:T(4,128)}) custom-call(f32[128,512]{1,0:T(8,128)S(1)} %get-tuple-element.15.q_ref, f32[128,2560]{1,0:T(8,128)S(1)} %get-tuple-element.16.rest_ref, f32[128,128]{1,0:T(8,128)S(1)} %get-tuple-element.17.gates_ref, ...), custom_call_target="tpu_custom_call" | custom-call | flops 33554432 | bytes 16777216 | tf_op jit(solution)/shard_map/tree_read/pallas_call | solution.py:127
  87.3 0.0 copy-done.3
  87.3 30.7 %spread.1 = bf16[256,512]{1,0:T(8,128)(2,1)S(1)} custom-call(bf16[128,1024]{1,0:T(8,128)(2,1)S(1)} %get-tuple-element.22.hid_ref, bf16[1024,512]{1,0:T(8,128)(2,1)S(1)} %copy-done.3), custom_call_target="tpu_custom_call" | custom-call | flops 1073741824 | bytes 1048576 | tf_op jit(solution)/shard_map/spread/pallas_call | solution.py:359
  118.1 0.7 copy.24
Async XLA Ops:
  0.6 78.0 %copy-start.1 = (s32[32,4]{0,1:T(4,128)S(1)}, s32[32,4]{0,1:T(4,128)}, u32[]{:S(2)}) copy-start(s32[32,4]{0,1:T(4,128)} %param.37) | copy-start | bytes 1540
  0.6 78.0 %copy-start = (f32[1024]{0:T(1024)S(1)}, f32[1024]{0:T(1024)}, u32[]{:S(2)}) copy-start(f32[1024]{0:T(1024)} %param.27) | copy-start | bytes 12292
  0.7 78.0 %copy-start.2 = (f32[16]{0:T(128)S(1)}, f32[16]{0:T(128)}, u32[]{:S(2)}) copy-start(f32[16]{0:T(128)} %param.26) | copy-start | bytes 196
  0.7 86.7 %copy-start.3 = (bf16[1024,512]{1,0:T(8,128)(2,1)S(1)}, bf16[1024,512]{1,0:T(8,128)(2,1)}, u32[]{:S(2)}) copy-start(bf16[1024,512]{1,0:T(8,128)(2,1)} %w_ref.1) | copy-start | bytes 3145732

commit v2 on v1

--- a/solution.py
+++ b/solution.py
@@ -353,7 +353,7 @@
     cols = weight.shape[1]
     kv = ny * nz
     per = kv // tp
-    cuts = 2
+    cuts = 4
     vmem = pl.BlockSpec(memory_space=pltpu.VMEM)
     dma = pltpu.SemaphoreType.DMA
     return pl.pallas_call(
@@ -753,21 +753,20 @@
         up_at, down_at = n - lag * z, n - lag * (nz - 1 - z)
         flow(True, up_at, False)
         flow(False, down_at, False)
-
-        @pl.when(n == close_at)
-        def _():
-            close_query()
-
-        @pl.when(jnp.logical_and(n >= 2, n < 2 + seqs // 2))
-        def _():
-            commit(2 * (n - 2))
-
-        @pl.when(n == product_at)
-        def _():
-            finish_query()
-
         flow(True, up_at, True)
         flow(False, down_at, True)
+
+        @pl.when(n == close_at)
+        def _():
+            close_query()
+
+        @pl.when(jnp.logical_and(n >= 2, n < 2 + seqs // 2))
+        def _():
+            commit(2 * (n - 2))
+
+        @pl.when(n == product_at)
+        def _():
+            finish_query()
 
         @pl.when(n == close_at)
         def _():

time: 119 us -> 118 us (level)
  no operation moved by 1% of the time
where the time goes in v2:
time: 118 us; the launch traced here: 117 us
  Pallas kernels  116 us (98%)
    pallas_call x1, Pallas kernels, gather_sums(): pl.pallas_call(functools.partial(gather_sums_kernel, ny, nz, 2), out_shap...  77.3 us
    pallas_call x1, Pallas kernels, spread_out(): pl.pallas_call(functools.partial(spread_kernel, ny, nz, tp, cuts), out_sh...  30 us
    pallas_call x1, Pallas kernels, tree_read(): pl.pallas_call(tree_kernel, out_shape=[pltpu.VMEM((rows, heads * DV), BF1...  8.62 us

profile of v2, /device:TPU:0, one launch (start us, length us, event | category | flops | bytes accessed | tf_op | source)
XLA Modules:
  0.0 117.4 jit_solution(6216954224183186416)
XLA Ops:
  0.6 0.0 copy-start.1
  0.6 0.0 copy-start
  0.7 0.0 copy-start.2
  0.7 0.0 copy-start.3
  0.7 77.3 %gather_sums.1 = (f32[128,512]{1,0:T(8,128)S(1)}, f32[128,2560]{1,0:T(8,128)S(1)}, f32[128,128]{1,0:T(8,128)S(1)}, f32[128,1024]{1,0:T(8,128)S(1)}, f32[32,4,128...) custom-call(bf16[1024,512]{1,0:T(8,128)(2,1)} %tok_hbm.1, f32[1,4096]{1,0:T(1,128)} %bitcast.14, ...), custom_call_target="tpu_custom_call" | custom-call | flops 3221225472 | bytes 19922944 | tf_op jit(solution)/shard_map/gather_sums/pallas_call | solution.py:880
  78.0 0.0 copy-done.1
  78.0 0.0 copy-done
  78.1 0.0 copy-done.2
  78.1 8.6 %tree_read.1 = (bf16[128,1024]{1,0:T(8,128)(2,1)S(1)}, f32[32,4,128,256]{3,2,1,0:T(8,128)}, f32[32,4,128]{2,1,0:T(4,128)}, f32[4,32]{1,0:T(4,128)}) custom-call(f32[128,512]{1,0:T(8,128)S(1)} %get-tuple-element.15.q_ref, f32[128,2560]{1,0:T(8,128)S(1)} %get-tuple-element.16.rest_ref, f32[128,128]{1,0:T(8,128)S(1)} %get-tuple-element.17.gates_ref, ...), custom_call_target="tpu_custom_call" | custom-call | flops 33554432 | bytes 16777216 | tf_op jit(solution)/shard_map/tree_read/pallas_call | solution.py:127
  86.7 0.0 copy-done.3
  86.7 30.0 %spread.1 = bf16[256,512]{1,0:T(8,128)(2,1)S(1)} custom-call(bf16[128,1024]{1,0:T(8,128)(2,1)S(1)} %get-tuple-element.22.hid_ref, bf16[1024,512]{1,0:T(8,128)(2,1)S(1)} %copy-done.3), custom_call_target="tpu_custom_call" | custom-call | flops 1073741824 | bytes 1048576 | tf_op jit(solution)/shard_map/spread/pallas_call | solution.py:359
  116.7 0.7 copy.24
Async XLA Ops:
  0.6 77.4 %copy-start.1 = (s32[32,4]{0,1:T(4,128)S(1)}, s32[32,4]{0,1:T(4,128)}, u32[]{:S(2)}) copy-start(s32[32,4]{0,1:T(4,128)} %param.37) | copy-start | bytes 1540
  0.6 77.4 %copy-start = (f32[1024]{0:T(1024)S(1)}, f32[1024]{0:T(1024)}, u32[]{:S(2)}) copy-start(f32[1024]{0:T(1024)} %param.27) | copy-start | bytes 12292
  0.7 77.4 %copy-start.2 = (f32[16]{0:T(128)S(1)}, f32[16]{0:T(128)}, u32[]{:S(2)}) copy-start(f32[16]{0:T(128)} %param.26) | copy-start | bytes 196
  0.7 86.0 %copy-start.3 = (bf16[1024,512]{1,0:T(8,128)(2,1)S(1)}, bf16[1024,512]{1,0:T(8,128)(2,1)}, u32[]{:S(2)}) copy-start(bf16[1024,512]{1,0:T(8,128)(2,1)} %w_ref.1) | copy-start | bytes 3145732
